TPU v7x, 32 devices: a whole 2x2x4 slice. The times are simulated.
32 devices in a mesh: ep: 8 (over z, x), tp: 4 (over y, core).
Axes of the slice: x: 2, y: 2, z: 4, core: 2. Of those that a mesh axis runs over, the one named last changes fastest.
Arguments:
- queries: bfloat16 [6144, 1024], P('ep', 'tp'), may hold values from -6.5 to 6.5
- keys: bfloat16 [6144, 1024], P('ep', 'tp'), may hold values from -6.5 to 6.5
- values: bfloat16 [6144, 1024], P('ep', 'tp'), may hold values from -6 to 6
- cum_gate: float32 [6144, 16], P('ep', 'tp'), may hold values from -770 to 0, as said below
- head_gain: float32 [1024], P('tp'), may hold values from 0.1 to 1.9
- moe_in: bfloat16 [1024, 2048], P('ep'), may hold values from -6 to 6
- ffn_gain: float32 [2048], replicated, may hold values from 0.1 to 1.9
- routes: int32 [1024, 4], P('ep'), may hold values from 0 to 31, all different within a row; in each aligned block of 128 rows (0 to 127, 128 to 255, ...) at most 24 rows name the same one
- route_weight: float32 [1024, 4], P('ep'), may hold values from 0.2 to 1.2
- expert_gate: bfloat16 [32, 1024, 2048], P('ep', 'tp'), may hold values from -0.125 to 0.125
- expert_up: bfloat16 [32, 1024, 2048], P('ep', 'tp'), may hold values from -0.125 to 0.125
- expert_down: bfloat16 [32, 1024, 2048], P('ep', 'tp'), may hold values from -0.25 to 0.25
- shared_gate: bfloat16 [512, 2048], P('tp'), may hold values from -0.125 to 0.125
- shared_up: bfloat16 [512, 2048], P('tp'), may hold values from -0.125 to 0.125
- shared_down: bfloat16 [512, 2048], P('tp'), may hold values from -0.375 to 0.375
Outputs:
- mixed: bfloat16 [6144, 1024], P('ep', 'tp')
- expert_out: bfloat16 [1024, 2048], P('ep', 'tp')
Inputs may be any that keep to these rules, and one draw needn't show every extreme that they name: `routes`: in each aligned block of 128 rows (the tokens of one index of ep) no expert is named by more than 24 rows, a bound that some block reaches; a row names 4 different experts. Each head's cum_gate never rises from one position to the next.
All inputs are finite; a program needn't handle non-finite values.
Results may differ from a plain program's by a relative error of at most 0.019.
Values may be sent and summed in bfloat16 or wider, within the bound.
A program may use at most 128 MiB of HBM per device.

v0:
```python
import math
import jax
import jax.numpy as jnp
from jax import lax
from jax.sharding import PartitionSpec as P

NORM_EPSILON = 1e-06


def keep_same(state_pair):
    return state_pair


def attend(queries, keys, values, cum_gate, head_gain):
    row_count, head_width = queries.shape
    head_count = cum_gate.shape[1]
    head_size = head_width // head_count
    score_scale = head_size ** (-0.5)
    first_row = lax.axis_index("ep") * row_count
    last_row = first_row + row_count - 1
    query_heads = queries.reshape(row_count, head_count, head_size)
    query_pos = first_row + jnp.arange(row_count, dtype=jnp.int32)
    query_gate = cum_gate.T
    all_gates = lax.all_gather(cum_gate, "ep", axis=0, tiled=True)
    start_state = (
        jnp.full((head_count, row_count), -1e30, jnp.float32),
        jnp.zeros((row_count, head_count, head_size), jnp.float32),
    )
    key_piece = lax.all_gather(keys, "ep", axis=0, tiled=True)
    value_piece = lax.all_gather(values, "ep", axis=0, tiled=True)
    piece_len = key_piece.shape[0]
    block_len = math.gcd(piece_len, 512)

    def visit(block_num, state_pair):
        offset = block_num * block_len

        def update(pair_in):
            running, weighted = pair_in
            key_block = lax.dynamic_slice_in_dim(key_piece, offset, block_len, 0).reshape(
                block_len, head_count, head_size
            )
            value_block = lax.dynamic_slice_in_dim(value_piece, offset, block_len, 0).reshape(
                block_len, head_count, head_size
            )
            key_gate = lax.dynamic_slice_in_dim(all_gates, offset, block_len, 0).T
            key_pos = offset + jnp.arange(block_len, dtype=jnp.int32)
            scores = (
                jnp.einsum(
                    "qhd,khd->hqk", query_heads, key_block, preferred_element_type=jnp.float32
                )
                * score_scale
            )
            scores = scores + query_gate[:, :, None] - key_gate[:, None, :]
            scores = jnp.where(key_pos[None, None, :] <= query_pos[None, :, None], scores, -jnp.inf)
            new_peak = jnp.maximum(running, jnp.max(scores, axis=2))
            weights = jnp.exp(scores - new_peak[:, :, None]).astype(jnp.bfloat16)
            shrink = jnp.exp(running - new_peak).T
            weighted = weighted * shrink[:, :, None] + jnp.einsum(
                "hqk,khd->qhd", weights, value_block, preferred_element_type=jnp.float32
            )
            return (new_peak, weighted)

        return lax.cond(offset <= last_row, update, keep_same, state_pair)

    running, weighted = lax.fori_loop(0, piece_len // block_len, visit, start_state)
    mean_square = jnp.mean(weighted * weighted, axis=2, keepdims=True)
    normed = (
        weighted * lax.rsqrt(mean_square + NORM_EPSILON) * head_gain.reshape(head_count, head_size)
    )
    return normed.reshape(row_count, head_width).astype(jnp.bfloat16)


def slot_index(route_rows, experts, capacity):
    flat_routes = route_rows.reshape(-1)
    agreement_tally = (
        flat_routes[:, None] == jnp.arange(experts, dtype=jnp.int32)[None, :]
    ).astype(jnp.int32)
    earlier = jnp.sum((jnp.cumsum(agreement_tally, axis=0) - 1) * agreement_tally, axis=1)
    return flat_routes * capacity + earlier


def experts_half(
    moe_in,
    ffn_gain,
    routes,
    route_weight,
    expert_gate,
    expert_up,
    expert_down,
    shared_gate,
    shared_up,
    shared_down,
):
    tokens, model_width = moe_in.shape
    choose = routes.shape[1]
    per_group = expert_gate.shape[0]
    groups = lax.axis_size("ep")
    experts = per_group * groups
    capacity = max(2, 3 * tokens * choose // (2 * experts))
    slice_width = model_width // lax.axis_size("tp")
    source = moe_in.astype(jnp.float32)
    normed = (
        source
        * lax.rsqrt(jnp.mean(source * source, axis=1, keepdims=True) + NORM_EPSILON)
        * ffn_gain
    ).astype(jnp.bfloat16)
    shared_hidden = (
        jax.nn.silu(
            jnp.einsum("td,fd->tf", normed, shared_gate, preferred_element_type=jnp.float32)
        )
        * jnp.einsum("td,fd->tf", normed, shared_up, preferred_element_type=jnp.float32)
    ).astype(jnp.bfloat16)
    shared_term = jnp.dot(shared_hidden, shared_down, preferred_element_type=jnp.float32)
    slot_ids = slot_index(routes, experts, capacity)
    owner_row = (
        jnp.full((experts * capacity,), tokens, jnp.int32)
        .at[slot_ids]
        .set(jnp.arange(tokens * choose, dtype=jnp.int32) // choose)
    )
    padded = jnp.concatenate([normed, jnp.zeros((1, model_width), normed.dtype)], axis=0)
    own_columns = lax.dynamic_slice_in_dim(
        padded, lax.axis_index("tp") * slice_width, slice_width, 1
    )
    arrived = lax.all_to_all(own_columns[owner_row], "ep", split_axis=0, concat_axis=0, tiled=True)
    column_piece = lax.all_gather(arrived, "tp", axis=1, tiled=True)
    piece_len = column_piece.shape[1]
    arranged = column_piece.reshape(groups, per_group, capacity, piece_len)
    gate_value = jnp.einsum(
        "slcd,lfd->slcf", arranged, expert_gate, preferred_element_type=jnp.float32
    )
    up_value = jnp.einsum("slcd,lfd->slcf", arranged, expert_up, preferred_element_type=jnp.float32)
    hidden = (jax.nn.silu(gate_value) * up_value).astype(jnp.bfloat16)
    expert_term = jnp.einsum(
        "slcf,lfd->slcd", hidden, expert_down, preferred_element_type=jnp.float32
    ).reshape(groups * per_group * capacity, model_width)
    expert_sum, shared_sum = (
        lax.psum_scatter(
            expert_term.astype(jnp.bfloat16), "tp", scatter_dimension=1, tiled=True
        ).astype(jnp.float32),
        lax.psum_scatter(
            shared_term.astype(jnp.bfloat16), "tp", scatter_dimension=1, tiled=True
        ).astype(jnp.float32),
    )
    returned = lax.all_to_all(
        expert_sum.astype(jnp.bfloat16), "ep", split_axis=0, concat_axis=0, tiled=True
    )
    picked = returned[slot_ids].reshape(tokens, choose, slice_width).astype(jnp.float32)
    routed = jnp.sum(picked * route_weight[:, :, None], axis=1)
    return (shared_sum + routed).astype(jnp.bfloat16)


def on_device(
    queries,
    keys,
    values,
    cum_gate,
    head_gain,
    moe_in,
    ffn_gain,
    routes,
    route_weight,
    expert_gate,
    expert_up,
    expert_down,
    shared_gate,
    shared_up,
    shared_down,
):
    mixed = attend(queries, keys, values, cum_gate, head_gain)
    expert_out = experts_half(
        moe_in,
        ffn_gain,
        routes,
        route_weight,
        expert_gate,
        expert_up,
        expert_down,
        shared_gate,
        shared_up,
        shared_down,
    )
    return (mixed, expert_out)


def solution(mesh):
    in_specs = (
        P("ep", "tp"),
        P("ep", "tp"),
        P("ep", "tp"),
        P("ep", "tp"),
        P("tp"),
        P("ep", None),
        P(),
        P("ep", None),
        P("ep", None),
        P("ep", "tp", None),
        P("ep", "tp", None),
        P("ep", "tp", None),
        P("tp", None),
        P("tp", None),
        P("tp", None),
    )
    out_specs = (P("ep", "tp"), P("ep", "tp"))
    return jax.shard_map(
        on_device, mesh=mesh, in_specs=in_specs, out_specs=out_specs, check_vma=False
    )
```

profile of v0, /device:TPU:27, one launch (start us, length us, event | category | flops | bytes accessed | tf_op | source)
XLA Modules:
  0.0 309.0 jit_solution(3351411150945842040)
XLA Ops:
  12.8 2.4 scatter_custom_fusion
  16.6 2.7 gather_fusion
  19.3 23.3 %all_to_all.24 = bf16[8,96,512]{2,1,0:T(8,128)(2,1)} all-to-all(bf16[8,96,512]{2,1,0:T(8,128)(2,1)S(1)} %bitcast.100), channel_id=1, replica_groups=mesh['ep'=8,'tp'=4] {'ep'}, dimensions={0} | all-to-all | bytes 1572864 | tf_op jit(solution)/shard_map/all_to_all | solution.py:124
  42.6 30.3 %all-gather.8.cloned.1.call-done = bf16[768,2048]{1,0:T(8,128)(2,1)} async-done(((bf16[768,512]{1,0:T(8,128)(2,1)}), bf16[768,2048]{1,0:T(8,128)(2,1)}) %all-gather.8.cloned.1.call-update) | async-done | bytes 3145744 | tf_op jit(solution)/shard_map/all_gather | solution.py:125
  73.0 4.7 %fusion.23 = f32[8,4,24,256]{3,2,0,1:T(8,128)S(1)} fusion(bf16[4,256,2048]{2,1,0:T(8,128)(2,1)} %param.28, bf16[8,4,24,2048]{3,2,1,0:T(8,128)(2,1)} %bitcast.109), kind=kOutput, calls=%fused_computation.33 | convolution fusion | flops 805306368 | bytes 8126464 | tf_op jit(solution)/shard_map/slcd,lfd->slcf/dot_general | solution.py:128
  77.6 8.5 %fusion.18 = bf16[8,4,24,2048]{3,2,0,1:T(8,128)(2,1)} fusion(bf16[4,256,2048]{2,1,0:T(8,128)(2,1)} %param.30, bf16[4,256,2048]{2,1,0:T(8,128)(2,1)} %param.29, bf16[8,4,24,2048]{3,2,1,0:T(8,128)(2,1)} %bitcast.110, f32[8,4,24,256]{3,2,0,1:T(8,128)S(1)} %fusion.23), kind=kOutput, calls=%fused_computation.27 | convolution fusion | flops 1613365248 | bytes 15466496 | tf_op jit(solution)/shard_map/slcf,lfd->slcd/dot_general | solution.py:133
  86.1 4.1 %copy.32 = bf16[8,4,24,2048]{3,2,1,0:T(8,128)(2,1)} copy(bf16[8,4,24,2048]{3,2,0,1:T(8,128)(2,1)} %fusion.18) | data formatting | bytes 6291456 | tf_op jit(solution)/shard_map/convert_element_type | solution.py:138
  92.3 35.2 %reduce-scatter.5.cloned.1.call-done = bf16[768,512]{1,0:T(8,128)(2,1)} async-done(((bf16[768,2048]{1,0:T(8,128)(2,1)}), bf16[768,512]{1,0:T(8,128)(2,1)}) %reduce-scatter.5.cloned.1.call-update) | async-done | bytes 786448 | tf_op jit(solution)/shard_map/reduce_scatter | solution.py:137
  127.5 5.4 %all-to-all-start.1 = ((bf16[8,96,512]{2,1,0:T(8,128)(2,1)}), bf16[8,96,512]{2,1,0:T(8,128)(2,1)S(1)}, u32[]{:S(2)}, u32[]{:S(2)}) async-start(bf16[8,96,512]{2,1,0:T(8,128)(2,1)} %bitcast.103), calls=%async_computation.3 | async-start | bytes 1572864 | tf_op jit(solution)/shard_map/all_to_all | solution.py:144
  135.3 44.6 %all_gather.13 = f32[6144,4]{0,1:T(4,128)S(1)} all-gather(f32[768,4]{0,1:T(4,128)S(1)} %copy-done.6), channel_id=1, replica_groups=mesh['ep'=8,'tp'=4] {'ep'}, dimensions={0}, use_global_device_ids=true | all-gather | bytes 110592 | tf_op jit(solution)/shard_map/all_gather | solution.py:24
  179.9 46.6 %all-gather.6.cloned.1.call-done = bf16[6144,256]{0,1:T(8,128)(2,1)} async-done(((bf16[768,256]{0,1:T(8,128)(2,1)}), bf16[6144,256]{0,1:T(8,128)(2,1)}) %all-gather.6.cloned.1.call-update) | async-done | bytes 3145744 | tf_op jit(solution)/shard_map/all_gather | solution.py:30
  226.6 69.5 %while.16 = (s32[]{:T(128)}, f32[4,768]{1,0:T(4,128)S(1)}, f32[768,4,64]{0,2,1:T(8,128)S(1)}, s32[]{:T(128)}, bf16[6144,256]{0,1:T(8,128)(2,1)}, /*index=5*/bf16...) while((s32[]{:T(128)}, f32[4,768]{1,0:T(4,128)S(1)}, ...), condition=%wide.region_4.5_spmd.clone, body=%wide.region_0.4_spmd.clone.sunk | while | flops 420745472 | bytes 17461568 | solution.py:65
  226.7 5.8 %conditional.3 = ((f32[4,768]{1,0:T(4,128)S(1)}, f32[768,4,64]{0,2,1:T(8,128)S(1)})) conditional(s32[]{:T(128)} %convert_element_type.106, (f32[4,768]{1,0:T(4,128)S(1)}, f32[768,4,64]{0,2,1:T(8,128)S(1)}) %tuple.50, (s32[]{:T(128)}, s32[]{:T(128)}, bf16[6144,256]{0,1:T(8,128)(2,1)}, bf16[768,4,64]{0,2,1:T(8,128)(2,1)S(1)}, f32[4,768]{1,0:T(4,128)S(1)}, ...), branch_computations={%region_1.0_spmd, %region_2.3_spmd} | conditional | flops 420745472 | bytes 17458250 | solution.py:63
  230.0 2.4 fusion.6
  232.5 5.7 %conditional.3 = ((f32[4,768]{1,0:T(4,128)S(1)}, f32[768,4,64]{0,2,1:T(8,128)S(1)})) conditional(s32[]{:T(128)} %convert_element_type.106, (f32[4,768]{1,0:T(4,128)S(1)}, f32[768,4,64]{0,2,1:T(8,128)S(1)}) %tuple.50, (s32[]{:T(128)}, s32[]{:T(128)}, bf16[6144,256]{0,1:T(8,128)(2,1)}, bf16[768,4,64]{0,2,1:T(8,128)(2,1)S(1)}, f32[4,768]{1,0:T(4,128)S(1)}, ...), branch_computations={%region_1.0_spmd, %region_2.3_spmd} | conditional | flops 420745472 | bytes 17458250 | solution.py:63
  235.8 2.4 fusion.6
  238.3 5.7 %conditional.3 = ((f32[4,768]{1,0:T(4,128)S(1)}, f32[768,4,64]{0,2,1:T(8,128)S(1)})) conditional(s32[]{:T(128)} %convert_element_type.106, (f32[4,768]{1,0:T(4,128)S(1)}, f32[768,4,64]{0,2,1:T(8,128)S(1)}) %tuple.50, (s32[]{:T(128)}, s32[]{:T(128)}, bf16[6144,256]{0,1:T(8,128)(2,1)}, bf16[768,4,64]{0,2,1:T(8,128)(2,1)S(1)}, f32[4,768]{1,0:T(4,128)S(1)}, ...), branch_computations={%region_1.0_spmd, %region_2.3_spmd} | conditional | flops 420745472 | bytes 17458250 | solution.py:63
  241.6 2.4 fusion.6
  244.0 5.7 %conditional.3 = ((f32[4,768]{1,0:T(4,128)S(1)}, f32[768,4,64]{0,2,1:T(8,128)S(1)})) conditional(s32[]{:T(128)} %convert_element_type.106, (f32[4,768]{1,0:T(4,128)S(1)}, f32[768,4,64]{0,2,1:T(8,128)S(1)}) %tuple.50, (s32[]{:T(128)}, s32[]{:T(128)}, bf16[6144,256]{0,1:T(8,128)(2,1)}, bf16[768,4,64]{0,2,1:T(8,128)(2,1)S(1)}, f32[4,768]{1,0:T(4,128)S(1)}, ...), branch_computations={%region_1.0_spmd, %region_2.3_spmd} | conditional | flops 420745472 | bytes 17458250 | solution.py:63
  249.8 5.7 %conditional.3 = ((f32[4,768]{1,0:T(4,128)S(1)}, f32[768,4,64]{0,2,1:T(8,128)S(1)})) conditional(s32[]{:T(128)} %convert_element_type.106, (f32[4,768]{1,0:T(4,128)S(1)}, f32[768,4,64]{0,2,1:T(8,128)S(1)}) %tuple.50, (s32[]{:T(128)}, s32[]{:T(128)}, bf16[6144,256]{0,1:T(8,128)(2,1)}, bf16[768,4,64]{0,2,1:T(8,128)(2,1)S(1)}, f32[4,768]{1,0:T(4,128)S(1)}, ...), branch_computations={%region_1.0_spmd, %region_2.3_spmd} | conditional | flops 420745472 | bytes 17458250 | solution.py:63
  253.2 2.4 fusion.6
  255.6 5.7 %conditional.3 = ((f32[4,768]{1,0:T(4,128)S(1)}, f32[768,4,64]{0,2,1:T(8,128)S(1)})) conditional(s32[]{:T(128)} %convert_element_type.106, (f32[4,768]{1,0:T(4,128)S(1)}, f32[768,4,64]{0,2,1:T(8,128)S(1)}) %tuple.50, (s32[]{:T(128)}, s32[]{:T(128)}, bf16[6144,256]{0,1:T(8,128)(2,1)}, bf16[768,4,64]{0,2,1:T(8,128)(2,1)S(1)}, f32[4,768]{1,0:T(4,128)S(1)}, ...), branch_computations={%region_1.0_spmd, %region_2.3_spmd} | conditional | flops 420745472 | bytes 17458250 | solution.py:63
  261.4 5.7 %conditional.3 = ((f32[4,768]{1,0:T(4,128)S(1)}, f32[768,4,64]{0,2,1:T(8,128)S(1)})) conditional(s32[]{:T(128)} %convert_element_type.106, (f32[4,768]{1,0:T(4,128)S(1)}, f32[768,4,64]{0,2,1:T(8,128)S(1)}) %tuple.50, (s32[]{:T(128)}, s32[]{:T(128)}, bf16[6144,256]{0,1:T(8,128)(2,1)}, bf16[768,4,64]{0,2,1:T(8,128)(2,1)S(1)}, f32[4,768]{1,0:T(4,128)S(1)}, ...), branch_computations={%region_1.0_spmd, %region_2.3_spmd} | conditional | flops 420745472 | bytes 17458250 | solution.py:63
  264.8 2.4 fusion.6
  267.2 5.7 %conditional.3 = ((f32[4,768]{1,0:T(4,128)S(1)}, f32[768,4,64]{0,2,1:T(8,128)S(1)})) conditional(s32[]{:T(128)} %convert_element_type.106, (f32[4,768]{1,0:T(4,128)S(1)}, f32[768,4,64]{0,2,1:T(8,128)S(1)}) %tuple.50, (s32[]{:T(128)}, s32[]{:T(128)}, bf16[6144,256]{0,1:T(8,128)(2,1)}, bf16[768,4,64]{0,2,1:T(8,128)(2,1)S(1)}, f32[4,768]{1,0:T(4,128)S(1)}, ...), branch_computations={%region_1.0_spmd, %region_2.3_spmd} | conditional | flops 420745472 | bytes 17458250 | solution.py:63
  270.6 2.4 fusion.6
  273.0 5.7 %conditional.3 = ((f32[4,768]{1,0:T(4,128)S(1)}, f32[768,4,64]{0,2,1:T(8,128)S(1)})) conditional(s32[]{:T(128)} %convert_element_type.106, (f32[4,768]{1,0:T(4,128)S(1)}, f32[768,4,64]{0,2,1:T(8,128)S(1)}) %tuple.50, (s32[]{:T(128)}, s32[]{:T(128)}, bf16[6144,256]{0,1:T(8,128)(2,1)}, bf16[768,4,64]{0,2,1:T(8,128)(2,1)S(1)}, f32[4,768]{1,0:T(4,128)S(1)}, ...), branch_computations={%region_1.0_spmd, %region_2.3_spmd} | conditional | flops 420745472 | bytes 17458250 | solution.py:63
  276.4 2.4 fusion.6
  278.8 5.7 %conditional.3 = ((f32[4,768]{1,0:T(4,128)S(1)}, f32[768,4,64]{0,2,1:T(8,128)S(1)})) conditional(s32[]{:T(128)} %convert_element_type.106, (f32[4,768]{1,0:T(4,128)S(1)}, f32[768,4,64]{0,2,1:T(8,128)S(1)}) %tuple.50, (s32[]{:T(128)}, s32[]{:T(128)}, bf16[6144,256]{0,1:T(8,128)(2,1)}, bf16[768,4,64]{0,2,1:T(8,128)(2,1)S(1)}, f32[4,768]{1,0:T(4,128)S(1)}, ...), branch_computations={%region_1.0_spmd, %region_2.3_spmd} | conditional | flops 420745472 | bytes 17458250 | solution.py:63
  284.6 5.7 %conditional.3 = ((f32[4,768]{1,0:T(4,128)S(1)}, f32[768,4,64]{0,2,1:T(8,128)S(1)})) conditional(s32[]{:T(128)} %convert_element_type.106, (f32[4,768]{1,0:T(4,128)S(1)}, f32[768,4,64]{0,2,1:T(8,128)S(1)}) %tuple.50, (s32[]{:T(128)}, s32[]{:T(128)}, bf16[6144,256]{0,1:T(8,128)(2,1)}, bf16[768,4,64]{0,2,1:T(8,128)(2,1)S(1)}, f32[4,768]{1,0:T(4,128)S(1)}, ...), branch_computations={%region_1.0_spmd, %region_2.3_spmd} | conditional | flops 420745472 | bytes 17458250 | solution.py:63
  287.9 2.4 fusion.6
  290.4 5.7 %conditional.3 = ((f32[4,768]{1,0:T(4,128)S(1)}, f32[768,4,64]{0,2,1:T(8,128)S(1)})) conditional(s32[]{:T(128)} %convert_element_type.106, (f32[4,768]{1,0:T(4,128)S(1)}, f32[768,4,64]{0,2,1:T(8,128)S(1)}) %tuple.50, (s32[]{:T(128)}, s32[]{:T(128)}, bf16[6144,256]{0,1:T(8,128)(2,1)}, bf16[768,4,64]{0,2,1:T(8,128)(2,1)S(1)}, f32[4,768]{1,0:T(4,128)S(1)}, ...), branch_computations={%region_1.0_spmd, %region_2.3_spmd} | conditional | flops 420745472 | bytes 17458250 | solution.py:63
  (169 shorter events, 65.3 us)
Async XLA Ops:
  8.0 125.3 %copy-start = (bf16[128,2048]{1,0:T(8,128)(2,1)S(1)}, bf16[128,2048]{1,0:T(8,128)(2,1)}, u32[]{:S(2)}) copy-start(bf16[128,2048]{1,0:T(8,128)(2,1)} %param.33) | copy-start | bytes 1572868
  8.0 65.0 %all-gather.8.cloned.1.call-start = ((), (), s32[]{:S(2)}) async-start(), calls=%async_computation.7 | async-start | bytes 3932160 | tf_op jit(solution)/shard_map/all_gather | solution.py:125
  42.6 84.9 %reduce-scatter.5.cloned.1.call-start = ((), (), s32[]{:S(2)}) async-start(), calls=%async_computation.8 | async-start | bytes 3932160 | tf_op jit(solution)/shard_map/reduce_scatter | solution.py:137
  86.1 4.2 %copy-start.3 = (bf16[768,256]{1,0:T(8,128)(2,1)S(1)}, bf16[768,256]{1,0:T(8,128)(2,1)}, u32[]{:S(2)}) copy-start(bf16[768,256]{1,0:T(8,128)(2,1)} %param.20) | copy-start | bytes 1179652
  86.1 5.2 %copy-start.4 = (bf16[768,256]{1,0:T(8,128)(2,1)S(1)}, bf16[768,256]{1,0:T(8,128)(2,1)}, u32[]{:S(2)}) copy-start(bf16[768,256]{1,0:T(8,128)(2,1)} %param.21) | copy-start | bytes 1179652
  90.2 42.8 %copy-start.1 = (bf16[128,2048]{1,0:T(8,128)(2,1)S(1)}, bf16[128,2048]{1,0:T(8,128)(2,1)}, u32[]{:S(2)}) copy-start(bf16[128,2048]{1,0:T(8,128)(2,1)} %param.31) | copy-start | bytes 1572868
  90.2 43.1 %copy-start.2 = (bf16[128,2048]{1,0:T(8,128)(2,1)S(1)}, bf16[128,2048]{1,0:T(8,128)(2,1)}, u32[]{:S(2)}) copy-start(bf16[128,2048]{1,0:T(8,128)(2,1)} %param.32) | copy-start | bytes 1572868
  90.2 44.7 %copy-start.5 = (bf16[768,256]{1,0:T(8,128)(2,1)S(1)}, bf16[768,256]{1,0:T(8,128)(2,1)}, u32[]{:S(2)}) copy-start(bf16[768,256]{1,0:T(8,128)(2,1)} %param.19) | copy-start | bytes 1179652
  90.2 44.8 %copy-start.8 = (f32[256]{0:T(256)S(1)}, f32[256]{0:T(256)}, u32[]{:S(2)}) copy-start(f32[256]{0:T(256)} %param.23) | copy-start | bytes 3076
  90.3 44.9 %copy-start.7 = (f32[128,4]{0,1:T(4,128)S(1)}, f32[128,4]{0,1:T(4,128)}, u32[]{:S(2)}) copy-start(f32[128,4]{0,1:T(4,128)} %param.27) | copy-start | bytes 6148
  90.3 45.0 %copy-start.6 = (f32[768,4]{0,1:T(4,128)S(1)}, f32[768,4]{0,1:T(4,128)}, u32[]{:S(2)}) copy-start(f32[768,4]{0,1:T(4,128)} %param.22) | copy-start | bytes 36868
  90.3 89.6 %all-gather.4.cloned.1.call-start = ((), (), s32[]{:S(2)}) async-start(), calls=%async_computation.4 | async-start | bytes 3538944 | tf_op jit(solution)/shard_map/all_gather | solution.py:29
  91.3 135.3 %all-gather.6.cloned.1.call-start = ((), (), s32[]{:S(2)}) async-start(), calls=%async_computation.5 | async-start | bytes 3538944 | tf_op jit(solution)/shard_map/all_gather | solution.py:30
  127.5 169.8 %all-to-all-start.1 = ((bf16[8,96,512]{2,1,0:T(8,128)(2,1)}), bf16[8,96,512]{2,1,0:T(8,128)(2,1)S(1)}, u32[]{:S(2)}, u32[]{:S(2)}) async-start(bf16[8,96,512]{2,1,0:T(8,128)(2,1)} %bitcast.103), calls=%async_computation.3 | async-start | bytes 1572864 | tf_op jit(solution)/shard_map/all_to_all | solution.py:144
  132.9 167.4 %reduce-scatter.3.cloned.1.call-start = ((), (), s32[]{:S(2)}) async-start(), calls=%async_computation.6 | async-start | bytes 655360 | tf_op jit(solution)/shard_map/reduce_scatter | solution.py:140
Sparse Core Ops, SparseCore 0:
  42.7 30.1 all-gather.7
  90.3 37.1 reduce-scatter.4
  136.2 22.2 reduce-scatter.2
Sparse Core Ops, SparseCore 1:
  93.6 71.5 all-gather.3
  167.2 59.4 all-gather.5
where the time goes:
time: 310 us; the launch traced here: 309 us
  waiting for transfers between devices  112 us (36%)
  blocking collectives  67.9 us (22%)
  matrix products  66.4 us (21%)
  local copies, waits for them, and re-layouts  29.2 us (9%)
  between operations  15.5 us (5%)
  other arithmetic  10.8 us (3%)
  starting transfers between devices  5.61 us (2%)
    all_gather x1, waiting for transfers between devices, attend(): value_piece = lax.all_gather(values, 'ep', axis=0, tiled=True)  46.6 us
    all_gather x1, blocking collectives, attend(): all_gates = lax.all_gather(cum_gate, 'ep', axis=0, tiled=True)  44.6 us
    reduce_scatter x1, waiting for transfers between devices, experts_half(): lax.psum_scatter(expert_term.astype(jnp.bfloat16), 'tp', scatter_dimensio...  35.2 us
    all_gather x1, waiting for transfers between devices, experts_half(): column_piece = lax.all_gather(arrived, 'tp', axis=1, tiled=True)  30.3 us
    dot_general x12, matrix products, update(): jnp.einsum('hqk,khd->qhd', weights, value_block, preferred_element_type=j...  28.6 us
    all_to_all x1, blocking collectives, experts_half(): lax.all_to_all(own_columns[owner_row], 'ep', split_axis=0, concat_axis=0,...  23.3 us
    dot_general x12, matrix products, update(): jnp.einsum('qhd,khd->hqk', query_heads, key_block, preferred_element_type...  22.8 us
    dynamic_slice x12, local copies, waits for them, and re-layouts, update(): lax.dynamic_slice_in_dim(value_piece, offset, block_len, 0)  12.9 us
  transfers between devices with their start and end apart: 6, of which 3 were waited for; matrix products, arithmetic and copies ran while one was open for 25% of the time, Pallas kernels for 0%

commit v1 on v0

--- a/solution.py
+++ b/solution.py
@@ -26,8 +26,11 @@
         jnp.full((head_count, row_count), -1e30, jnp.float32),
         jnp.zeros((row_count, head_count, head_size), jnp.float32),
     )
-    key_piece = lax.all_gather(keys, "ep", axis=0, tiled=True)
-    value_piece = lax.all_gather(values, "ep", axis=0, tiled=True)
+    key_piece, value_piece = jnp.split(
+        lax.all_gather(jnp.concatenate([keys, values], axis=1), "ep", axis=0, tiled=True),
+        [keys.shape[1]],
+        axis=1,
+    )
     piece_len = key_piece.shape[0]
     block_len = math.gcd(piece_len, 512)
 

time: 310 us -> 292 us (0.942)
  blocking collectives: 67.9 us -> 48.9 us
  local copies, waits for them, and re-layouts: 29.2 us -> 34 us
  waiting for transfers between devices: 112 us -> 108 us
    reduce_scatter x1, waiting for transfers between devices: 35.2 us -> 7.8 us  [experts_half(): lax.psum_scatter(expert_term.astype(jnp.bfloat16), 'tp', scatter_dimensio...]
    all_gather x2 -> x1, waiting for transfers between devices: 46.7 us -> 69.7 us  [attend(): lax.all_gather(jnp.concatenate([keys, values], axis=1), 'ep', axis=0, til...]
    all_gather x1, blocking collectives: 44.6 us -> 25.6 us  [attend(): all_gates = lax.all_gather(cum_gate, 'ep', axis=0, tiled=True)]
    split x0 -> x1, local copies, waits for them, and re-layouts: none -> 6.25 us  [attend(): jnp.split(lax.all_gather(jnp.concatenate([keys, values], axis=1), 'ep', a...]
  transfers between devices with their start and end apart: 6 -> 5, of which waited for: 3 -> 3; matrix products, arithmetic and copies ran while one was open for 25% -> 28% of each run, Pallas kernels for 0% -> 0%
where the time goes in v1:
time: 292 us; the launch traced here: 291 us
  waiting for transfers between devices  108 us (37%)
  matrix products  66.4 us (23%)
  blocking collectives  48.9 us (17%)
  local copies, waits for them, and re-layouts  34 us (12%)
  between operations  15.5 us (5%)
  other arithmetic  11.7 us (4%)
  starting transfers between devices  5.6 us (2%)
    all_gather x1, waiting for transfers between devices, attend(): lax.all_gather(jnp.concatenate([keys, values], axis=1), 'ep', axis=0, til...  69.7 us
    all_gather x1, waiting for transfers between devices, experts_half(): column_piece = lax.all_gather(arrived, 'tp', axis=1, tiled=True)  30.3 us
    dot_general x12, matrix products, update(): jnp.einsum('hqk,khd->qhd', weights, value_block, preferred_element_type=j...  28.6 us
    all_gather x1, blocking collectives, attend(): all_gates = lax.all_gather(cum_gate, 'ep', axis=0, tiled=True)  25.6 us
    all_to_all x1, blocking collectives, experts_half(): lax.all_to_all(own_columns[owner_row], 'ep', split_axis=0, concat_axis=0,...  23.3 us
    dot_general x12, matrix products, update(): jnp.einsum('qhd,khd->hqk', query_heads, key_block, preferred_element_type...  22.8 us
    dynamic_slice x12, local copies, waits for them, and re-layouts, update(): lax.dynamic_slice_in_dim(value_piece, offset, block_len, 0)  12.9 us
    dot_general x1, matrix products, experts_half(): jnp.einsum('slcf,lfd->slcd', hidden, expert_down, preferred_element_type=...  8.52 us
  transfers between devices with their start and end apart: 5, of which 3 were waited for; matrix products, arithmetic and copies ran while one was open for 28% of the time, Pallas kernels for 0%

profile of v1, /device:TPU:27, one launch (start us, length us, event | category | flops | bytes accessed | tf_op | source)
XLA Modules:
  0.0 291.4 jit_solution(9906781773303249806)
XLA Ops:
  12.8 2.4 scatter_custom_fusion
  16.6 2.7 gather_fusion
  19.3 23.3 %all_to_all.24 = bf16[8,96,512]{2,1,0:T(8,128)(2,1)} all-to-all(bf16[8,96,512]{2,1,0:T(8,128)(2,1)S(1)} %bitcast.100), channel_id=1, replica_groups=mesh['ep'=8,'tp'=4] {'ep'}, dimensions={0} | all-to-all | bytes 1572864 | tf_op jit(solution)/shard_map/all_to_all | solution.py:127
  42.6 30.3 %all-gather.5.cloned.1.call-done = bf16[768,2048]{1,0:T(8,128)(2,1)} async-done(((bf16[768,512]{1,0:T(8,128)(2,1)}), bf16[768,2048]{1,0:T(8,128)(2,1)}) %all-gather.5.cloned.1.call-update) | async-done | bytes 3145744 | tf_op jit(solution)/shard_map/all_gather | solution.py:128
  73.0 4.7 %fusion.23 = f32[8,4,24,256]{3,2,0,1:T(8,128)S(1)} fusion(bf16[4,256,2048]{2,1,0:T(8,128)(2,1)} %param.28, bf16[8,4,24,2048]{3,2,1,0:T(8,128)(2,1)} %bitcast.109), kind=kOutput, calls=%fused_computation.33 | convolution fusion | flops 805306368 | bytes 8126464 | tf_op jit(solution)/shard_map/slcd,lfd->slcf/dot_general | solution.py:131
  77.6 8.5 %fusion.18 = bf16[8,4,24,2048]{3,2,0,1:T(8,128)(2,1)} fusion(bf16[4,256,2048]{2,1,0:T(8,128)(2,1)} %param.30, bf16[4,256,2048]{2,1,0:T(8,128)(2,1)} %param.29, bf16[8,4,24,2048]{3,2,1,0:T(8,128)(2,1)} %bitcast.110, f32[8,4,24,256]{3,2,0,1:T(8,128)S(1)} %fusion.23), kind=kOutput, calls=%fused_computation.27 | convolution fusion | flops 1613365248 | bytes 15466496 | tf_op jit(solution)/shard_map/slcf,lfd->slcd/dot_general | solution.py:136
  86.2 4.1 %copy.32 = bf16[8,4,24,2048]{3,2,1,0:T(8,128)(2,1)} copy(bf16[8,4,24,2048]{3,2,0,1:T(8,128)(2,1)} %fusion.18) | data formatting | bytes 6291456 | tf_op jit(solution)/shard_map/convert_element_type | solution.py:141
  93.9 25.6 %all_gather.10 = f32[6144,4]{0,1:T(4,128)S(1)} all-gather(f32[768,4]{0,1:T(4,128)S(1)} %copy-done.6), channel_id=1, replica_groups=mesh['ep'=8,'tp'=4] {'ep'}, dimensions={0}, use_global_device_ids=true | all-gather | bytes 110592 | tf_op jit(solution)/shard_map/all_gather | solution.py:24
  119.7 7.8 %reduce-scatter.5.cloned.1.call-done = bf16[768,512]{1,0:T(8,128)(2,1)} async-done(((bf16[768,2048]{1,0:T(8,128)(2,1)}), bf16[768,512]{1,0:T(8,128)(2,1)}) %reduce-scatter.5.cloned.1.call-update) | async-done | bytes 786448 | tf_op jit(solution)/shard_map/reduce_scatter | solution.py:140
  127.5 5.4 %all-to-all-start.1 = ((bf16[8,96,512]{2,1,0:T(8,128)(2,1)}), bf16[8,96,512]{2,1,0:T(8,128)(2,1)S(1)}, u32[]{:S(2)}, u32[]{:S(2)}) async-start(bf16[8,96,512]{2,1,0:T(8,128)(2,1)} %bitcast.103), calls=%async_computation.3 | async-start | bytes 1572864 | tf_op jit(solution)/shard_map/all_to_all | solution.py:147
  133.0 69.7 %all-gather.3.cloned.1.call-done = bf16[6144,512]{0,1:T(8,128)(2,1)} async-done(((bf16[768,512]{0,1:T(8,128)(2,1)}), bf16[6144,512]{0,1:T(8,128)(2,1)}) %all-gather.3.cloned.1.call-update) | async-done | bytes 6291472 | tf_op jit(solution)/shard_map/all_gather | solution.py:30
  202.7 6.2 %fusion.73 = (bf16[6144,256]{0,1:T(8,128)(2,1)}, bf16[6144,256]{0,1:T(8,128)(2,1)}) fusion(bf16[6144,512]{0,1:T(8,128)(2,1)} %all-gather.3.cloned.1.call-done), kind=kLoop, calls=%fused_computation.86 | loop fusion | bytes 12582912 | tf_op jit(solution)/shard_map/split | solution.py:29
  209.0 69.5 %while.16 = (s32[]{:T(128)}, f32[4,768]{1,0:T(4,128)S(1)}, f32[768,4,64]{0,2,1:T(8,128)S(1)}, s32[]{:T(128)}, bf16[6144,256]{0,1:T(8,128)(2,1)}, /*index=5*/bf16...) while((s32[]{:T(128)}, f32[4,768]{1,0:T(4,128)S(1)}, ...), condition=%wide.region_4.5_spmd.clone, body=%wide.region_0.4_spmd.clone.sunk | while | flops 420745472 | bytes 17461568 | solution.py:68
  209.0 5.8 %conditional.3 = ((f32[4,768]{1,0:T(4,128)S(1)}, f32[768,4,64]{0,2,1:T(8,128)S(1)})) conditional(s32[]{:T(128)} %convert_element_type.106, (f32[4,768]{1,0:T(4,128)S(1)}, f32[768,4,64]{0,2,1:T(8,128)S(1)}) %tuple.51, (s32[]{:T(128)}, s32[]{:T(128)}, bf16[6144,256]{0,1:T(8,128)(2,1)}, bf16[768,4,64]{0,2,1:T(8,128)(2,1)S(1)}, f32[4,768]{1,0:T(4,128)S(1)}, ...), branch_computations={%region_1.0_spmd, %region_2.3_spmd} | conditional | flops 420745472 | bytes 17458250 | solution.py:66
  212.4 2.4 fusion.6
  214.8 5.7 %conditional.3 = ((f32[4,768]{1,0:T(4,128)S(1)}, f32[768,4,64]{0,2,1:T(8,128)S(1)})) conditional(s32[]{:T(128)} %convert_element_type.106, (f32[4,768]{1,0:T(4,128)S(1)}, f32[768,4,64]{0,2,1:T(8,128)S(1)}) %tuple.51, (s32[]{:T(128)}, s32[]{:T(128)}, bf16[6144,256]{0,1:T(8,128)(2,1)}, bf16[768,4,64]{0,2,1:T(8,128)(2,1)S(1)}, f32[4,768]{1,0:T(4,128)S(1)}, ...), branch_computations={%region_1.0_spmd, %region_2.3_spmd} | conditional | flops 420745472 | bytes 17458250 | solution.py:66
  220.6 5.7 %conditional.3 = ((f32[4,768]{1,0:T(4,128)S(1)}, f32[768,4,64]{0,2,1:T(8,128)S(1)})) conditional(s32[]{:T(128)} %convert_element_type.106, (f32[4,768]{1,0:T(4,128)S(1)}, f32[768,4,64]{0,2,1:T(8,128)S(1)}) %tuple.51, (s32[]{:T(128)}, s32[]{:T(128)}, bf16[6144,256]{0,1:T(8,128)(2,1)}, bf16[768,4,64]{0,2,1:T(8,128)(2,1)S(1)}, f32[4,768]{1,0:T(4,128)S(1)}, ...), branch_computations={%region_1.0_spmd, %region_2.3_spmd} | conditional | flops 420745472 | bytes 17458250 | solution.py:66
  224.0 2.4 fusion.6
  226.4 5.7 %conditional.3 = ((f32[4,768]{1,0:T(4,128)S(1)}, f32[768,4,64]{0,2,1:T(8,128)S(1)})) conditional(s32[]{:T(128)} %convert_element_type.106, (f32[4,768]{1,0:T(4,128)S(1)}, f32[768,4,64]{0,2,1:T(8,128)S(1)}) %tuple.51, (s32[]{:T(128)}, s32[]{:T(128)}, bf16[6144,256]{0,1:T(8,128)(2,1)}, bf16[768,4,64]{0,2,1:T(8,128)(2,1)S(1)}, f32[4,768]{1,0:T(4,128)S(1)}, ...), branch_computations={%region_1.0_spmd, %region_2.3_spmd} | conditional | flops 420745472 | bytes 17458250 | solution.py:66
  229.7 2.4 fusion.6
  232.2 5.7 %conditional.3 = ((f32[4,768]{1,0:T(4,128)S(1)}, f32[768,4,64]{0,2,1:T(8,128)S(1)})) conditional(s32[]{:T(128)} %convert_element_type.106, (f32[4,768]{1,0:T(4,128)S(1)}, f32[768,4,64]{0,2,1:T(8,128)S(1)}) %tuple.51, (s32[]{:T(128)}, s32[]{:T(128)}, bf16[6144,256]{0,1:T(8,128)(2,1)}, bf16[768,4,64]{0,2,1:T(8,128)(2,1)S(1)}, f32[4,768]{1,0:T(4,128)S(1)}, ...), branch_computations={%region_1.0_spmd, %region_2.3_spmd} | conditional | flops 420745472 | bytes 17458250 | solution.py:66
  235.5 2.4 fusion.6
  238.0 5.7 %conditional.3 = ((f32[4,768]{1,0:T(4,128)S(1)}, f32[768,4,64]{0,2,1:T(8,128)S(1)})) conditional(s32[]{:T(128)} %convert_element_type.106, (f32[4,768]{1,0:T(4,128)S(1)}, f32[768,4,64]{0,2,1:T(8,128)S(1)}) %tuple.51, (s32[]{:T(128)}, s32[]{:T(128)}, bf16[6144,256]{0,1:T(8,128)(2,1)}, bf16[768,4,64]{0,2,1:T(8,128)(2,1)S(1)}, f32[4,768]{1,0:T(4,128)S(1)}, ...), branch_computations={%region_1.0_spmd, %region_2.3_spmd} | conditional | flops 420745472 | bytes 17458250 | solution.py:66
  243.7 5.7 %conditional.3 = ((f32[4,768]{1,0:T(4,128)S(1)}, f32[768,4,64]{0,2,1:T(8,128)S(1)})) conditional(s32[]{:T(128)} %convert_element_type.106, (f32[4,768]{1,0:T(4,128)S(1)}, f32[768,4,64]{0,2,1:T(8,128)S(1)}) %tuple.51, (s32[]{:T(128)}, s32[]{:T(128)}, bf16[6144,256]{0,1:T(8,128)(2,1)}, bf16[768,4,64]{0,2,1:T(8,128)(2,1)S(1)}, f32[4,768]{1,0:T(4,128)S(1)}, ...), branch_computations={%region_1.0_spmd, %region_2.3_spmd} | conditional | flops 420745472 | bytes 17458250 | solution.py:66
  247.1 2.4 fusion.6
  249.5 5.7 %conditional.3 = ((f32[4,768]{1,0:T(4,128)S(1)}, f32[768,4,64]{0,2,1:T(8,128)S(1)})) conditional(s32[]{:T(128)} %convert_element_type.106, (f32[4,768]{1,0:T(4,128)S(1)}, f32[768,4,64]{0,2,1:T(8,128)S(1)}) %tuple.51, (s32[]{:T(128)}, s32[]{:T(128)}, bf16[6144,256]{0,1:T(8,128)(2,1)}, bf16[768,4,64]{0,2,1:T(8,128)(2,1)S(1)}, f32[4,768]{1,0:T(4,128)S(1)}, ...), branch_computations={%region_1.0_spmd, %region_2.3_spmd} | conditional | flops 420745472 | bytes 17458250 | solution.py:66
  255.3 5.7 %conditional.3 = ((f32[4,768]{1,0:T(4,128)S(1)}, f32[768,4,64]{0,2,1:T(8,128)S(1)})) conditional(s32[]{:T(128)} %convert_element_type.106, (f32[4,768]{1,0:T(4,128)S(1)}, f32[768,4,64]{0,2,1:T(8,128)S(1)}) %tuple.51, (s32[]{:T(128)}, s32[]{:T(128)}, bf16[6144,256]{0,1:T(8,128)(2,1)}, bf16[768,4,64]{0,2,1:T(8,128)(2,1)S(1)}, f32[4,768]{1,0:T(4,128)S(1)}, ...), branch_computations={%region_1.0_spmd, %region_2.3_spmd} | conditional | flops 420745472 | bytes 17458250 | solution.py:66
  258.7 2.4 fusion.6
  261.1 5.7 %conditional.3 = ((f32[4,768]{1,0:T(4,128)S(1)}, f32[768,4,64]{0,2,1:T(8,128)S(1)})) conditional(s32[]{:T(128)} %convert_element_type.106, (f32[4,768]{1,0:T(4,128)S(1)}, f32[768,4,64]{0,2,1:T(8,128)S(1)}) %tuple.51, (s32[]{:T(128)}, s32[]{:T(128)}, bf16[6144,256]{0,1:T(8,128)(2,1)}, bf16[768,4,64]{0,2,1:T(8,128)(2,1)S(1)}, f32[4,768]{1,0:T(4,128)S(1)}, ...), branch_computations={%region_1.0_spmd, %region_2.3_spmd} | conditional | flops 420745472 | bytes 17458250 | solution.py:66
  266.9 5.7 %conditional.3 = ((f32[4,768]{1,0:T(4,128)S(1)}, f32[768,4,64]{0,2,1:T(8,128)S(1)})) conditional(s32[]{:T(128)} %convert_element_type.106, (f32[4,768]{1,0:T(4,128)S(1)}, f32[768,4,64]{0,2,1:T(8,128)S(1)}) %tuple.51, (s32[]{:T(128)}, s32[]{:T(128)}, bf16[6144,256]{0,1:T(8,128)(2,1)}, bf16[768,4,64]{0,2,1:T(8,128)(2,1)S(1)}, f32[4,768]{1,0:T(4,128)S(1)}, ...), branch_computations={%region_1.0_spmd, %region_2.3_spmd} | conditional | flops 420745472 | bytes 17458250 | solution.py:66
  270.3 2.4 fusion.6
  272.7 5.7 %conditional.3 = ((f32[4,768]{1,0:T(4,128)S(1)}, f32[768,4,64]{0,2,1:T(8,128)S(1)})) conditional(s32[]{:T(128)} %convert_element_type.106, (f32[4,768]{1,0:T(4,128)S(1)}, f32[768,4,64]{0,2,1:T(8,128)S(1)}) %tuple.51, (s32[]{:T(128)}, s32[]{:T(128)}, bf16[6144,256]{0,1:T(8,128)(2,1)}, bf16[768,4,64]{0,2,1:T(8,128)(2,1)S(1)}, f32[4,768]{1,0:T(4,128)S(1)}, ...), branch_computations={%region_1.0_spmd, %region_2.3_spmd} | conditional | flops 420745472 | bytes 17458250 | solution.py:66
  (168 shorter events, 67.1 us)
Async XLA Ops:
  8.0 84.1 %copy-start = (bf16[128,2048]{1,0:T(8,128)(2,1)S(1)}, bf16[128,2048]{1,0:T(8,128)(2,1)}, u32[]{:S(2)}) copy-start(bf16[128,2048]{1,0:T(8,128)(2,1)} %param.33) | copy-start | bytes 1572868
  8.0 65.0 %all-gather.5.cloned.1.call-start = ((), (), s32[]{:S(2)}) async-start(), calls=%async_computation.6 | async-start | bytes 3932160 | tf_op jit(solution)/shard_map/all_gather | solution.py:128
  42.6 84.9 %reduce-scatter.5.cloned.1.call-start = ((), (), s32[]{:S(2)}) async-start(), calls=%async_computation.7 | async-start | bytes 3932160 | tf_op jit(solution)/shard_map/reduce_scatter | solution.py:140
  86.1 4.2 %copy-start.3 = (bf16[768,256]{1,0:T(8,128)(2,1)S(1)}, bf16[768,256]{1,0:T(8,128)(2,1)}, u32[]{:S(2)}) copy-start(bf16[768,256]{1,0:T(8,128)(2,1)} %param.21) | copy-start | bytes 1179652
  86.1 4.4 %copy-start.4 = (bf16[768,256]{1,0:T(8,128)(2,1)S(1)}, bf16[768,256]{1,0:T(8,128)(2,1)}, u32[]{:S(2)}) copy-start(bf16[768,256]{1,0:T(8,128)(2,1)} %param.20) | copy-start | bytes 1179652
  90.2 1.5 copy-start.1
  90.2 1.8 copy-start.2
  90.3 3.6 %copy-start.6 = (f32[768,4]{0,1:T(4,128)S(1)}, f32[768,4]{0,1:T(4,128)}, u32[]{:S(2)}) copy-start(f32[768,4]{0,1:T(4,128)} %param.22) | copy-start | bytes 36868
  90.3 29.3 %copy-start.8 = (f32[256]{0:T(256)S(1)}, f32[256]{0:T(256)}, u32[]{:S(2)}) copy-start(f32[256]{0:T(256)} %param.23) | copy-start | bytes 3076
  90.3 29.3 %copy-start.7 = (f32[128,4]{0,1:T(4,128)S(1)}, f32[128,4]{0,1:T(4,128)}, u32[]{:S(2)}) copy-start(f32[128,4]{0,1:T(4,128)} %param.27) | copy-start | bytes 6148
  90.3 112.4 %all-gather.3.cloned.1.call-start = ((), (), s32[]{:S(2)}) async-start(), calls=%async_computation.4 | async-start | bytes 7077888 | tf_op jit(solution)/shard_map/all_gather | solution.py:30
  90.7 3.0 %copy-start.5 = (bf16[768,256]{1,0:T(8,128)(2,1)S(1)}, bf16[768,256]{1,0:T(8,128)(2,1)}, u32[]{:S(2)}) copy-start(bf16[768,256]{1,0:T(8,128)(2,1)} %param.19) | copy-start | bytes 1179652
  91.7 190.9 %reduce-scatter.3.cloned.1.call-start = ((), (), s32[]{:S(2)}) async-start(), calls=%async_computation.5 | async-start | bytes 655360 | tf_op jit(solution)/shard_map/reduce_scatter | solution.py:143
  127.5 152.1 %all-to-all-start.1 = ((bf16[8,96,512]{2,1,0:T(8,128)(2,1)}), bf16[8,96,512]{2,1,0:T(8,128)(2,1)S(1)}, u32[]{:S(2)}, u32[]{:S(2)}) async-start(bf16[8,96,512]{2,1,0:T(8,128)(2,1)} %bitcast.103), calls=%async_computation.3 | async-start | bytes 1572864 | tf_op jit(solution)/shard_map/all_to_all | solution.py:147
Sparse Core Ops, SparseCore 0:
  42.7 30.1 all-gather.4
  90.4 37.1 reduce-scatter.4
  130.0 21.6 reduce-scatter.2
Sparse Core Ops, SparseCore 1:
  93.0 109.6 all-gather.2
